TPU v7x, 256 devices: a whole 4x4x8 slice. The times are simulated.
256 devices in a mesh: sp: 32 (over z, x), tp: 8 (over y, core).
Axes of the slice: x: 4, y: 4, z: 8, core: 2. Of those that a mesh axis runs over, the one named last changes fastest.
Arguments:
- resid: bfloat16 [12288, 2048], P(('sp', 'tp')), may hold values from -6 to 6
- queries: bfloat16 [12288, 1024], P('sp', 'tp'), may hold values from -6 to 6
- keys: bfloat16 [12288, 1024], P('sp', 'tp'), may hold values from -6 to 6
- values: bfloat16 [12288, 1024], P('sp', 'tp'), may hold values from -6 to 6
- decay_input_part: bfloat16 [12288, 1024], P('sp', 'tp'), may hold values from -4 to 4
- decay_channel_offset: float32 [1024], P('tp'), may hold values from -16 to -2
- decay_head_extra: float32 [12288, 16], P('sp', 'tp'), may hold values from 0 to 0.7
- correction_rate_input: bfloat16 [12288, 1024], P('sp', 'tp'), may hold values from -6 to 6
- correction_rate_offset: float32 [1024], P('tp'), may hold values from -0.4 to 1
- head_norm_gain: float32 [1024], P('tp'), may hold values from 0.1 to 1.9
- mixer_output_weight: bfloat16 [1024, 2048], replicated, may hold values from -0.1875 to 0.1875
- feedforward_norm_gain: float32 [2048], replicated, may hold values from 0.1 to 1.9
- gate_weight: bfloat16 [2048, 5632], P('sp', 'tp'), may hold values from -0.125 to 0.125
- up_weight: bfloat16 [2048, 5632], P('sp', 'tp'), may hold values from -0.125 to 0.125
- down_weight: bfloat16 [5632, 2048], P('tp', 'sp'), may hold values from -0.078125 to 0.078125
Outputs:
- result: bfloat16 [12288, 2048], P(('sp', 'tp'))
All inputs are finite; a program needn't handle non-finite values.
Results may differ from a plain program's by a relative error of at most 0.014.
Values may be sent and summed in bfloat16 or wider, within the bound.
No kernel may reach another device: no remote copies, remote signals or barrier semaphores. Data moves between devices by JAX's collectives and lax.ppermute only.
A program may use at most 64 MiB of HBM per device.

v0:
```python
import jax
import jax.numpy as jnp
from jax import lax
from jax.sharding import Mesh
from jax.sharding import PartitionSpec as P

HEAD = 64
BLK = 16
SP = ("sp_0", "sp_1")
SP_TP = ("sp_0", "sp_1", "tp")


def nothing_yet(array, identity):
    return jax.tree.map(
        lambda a, e: jnp.broadcast_to(jnp.asarray(e, a.dtype), a.shape), array, identity
    )


def gathered_once(array, axis):
    leaves = jax.tree.leaves(array)
    sequence = sorted(range(len(leaves)), key=lambda k: -leaves[k].size)
    width = (1, *leaves[sequence[0]].shape)[-1]
    lines = [
        jnp.pad(leaves[k].reshape(-1), (0, -leaves[k].size % width)).reshape(-1, width)
        for k in sequence
    ]
    both, at, found = (lax.all_gather(jnp.concatenate(lines), axis), 0, {})
    for k, line in zip(sequence, lines):
        piece = both[:, at : at + len(line)].reshape(len(both), -1)
        found[k] = piece[:, : leaves[k].size].reshape(-1, *leaves[k].shape)
        at += len(line)
    numbers = iter(range(len(leaves)))
    return jax.tree.map(lambda _: found[next(numbers)], array)


def entering(array, axes, combine, identity):
    before = start = nothing_yet(array, identity)
    total = array
    for axis in reversed(axes):
        count, index = (lax.axis_size(axis), lax.axis_index(axis))
        pieces = gathered_once(
            jax.tree.map(
                lambda part, kind: part.astype(kind),
                total,
                jax.tree.map(lambda a: jnp.bfloat16 if a.dtype == jnp.float32 else a.dtype, array),
            ),
            axis,
        )
        inside, total = (start, start)
        for k in range(count):
            passed = k < index
            total = combine(
                total, jax.tree.map(lambda part, own: part[k].astype(own.dtype), pieces, array)
            )
            inside = jax.tree.map(lambda new, old: jnp.where(passed, new, old), total, inside)
        before = combine(inside, before)
    return before


def joined_along(pieces, dim):
    pieces = jnp.moveaxis(pieces, 0, dim)
    lengths = pieces.shape
    return pieces.reshape(*lengths[:dim], lengths[dim] * lengths[dim + 1], *lengths[dim + 2 :])


def from_everyone(array, axis):
    copies = jnp.broadcast_to(array, (lax.axis_size(axis), *array.shape))
    return lax.all_to_all(copies, axis, split_axis=0, concat_axis=0, tiled=True)


def gathered_copies(array, axis, dim):
    return joined_along(from_everyone(array, axis), dim)


def sent_together(arrays, axis, dim, along):
    both = jnp.concatenate(arrays, axis=along)
    whole, at, outs = (lax.all_gather(both, axis, axis=dim, tiled=True), 0, [])
    for a in arrays:
        outs.append(lax.slice_in_dim(whole, at, at + a.shape[along], axis=along))
        at += a.shape[along]
    return tuple(outs)


def whole_of(array, axes, dim):
    whole = array
    for number in range(len(axes) - 1, -1, -1):
        whole = lax.all_gather(whole, axes[number], axis=dim, tiled=True)
    return whole


def cut_along(array, dim, count):
    before, after = (array.shape[:dim], array.shape[dim + 1 :])
    return jnp.moveaxis(array.reshape(*before, count, -1, *after), dim, 0)


def sent_and_summed(array, axis, dim):
    count = lax.axis_size(axis)
    pieces = lax.all_to_all(cut_along(array, dim, count), axis, 0, 0, tiled=True)
    return jnp.sum(pieces.astype(jnp.float32), axis=0)


def matmul(left, right):
    return jnp.einsum("...ij,...jk->...ik", left, right, precision=lax.Precision.HIGHEST)


def combine(earlier, later):
    return (matmul(earlier[0], later[0]), matmul(earlier[1], later[0]) + later[1])


def block_step(carry, inputs):
    state, trans = carry
    query_t, decay_t, key_t, value_t, unit_t, lrate_t = inputs
    lifted = -unit_t
    state_dir = jnp.einsum("bhvk,bhk->bhv", state, lifted, precision=lax.Precision.HIGHEST)
    trans_dir = jnp.einsum("bhjk,bhk->bhj", trans, lifted, precision=lax.Precision.HIGHEST)
    scaled = unit_t * lrate_t
    state = (
        state * decay_t[:, :, None, :]
        + state_dir[..., None] * scaled[:, :, None, :]
        + value_t[..., None] * key_t[:, :, None, :]
    )
    trans = trans * decay_t[:, :, None, :] + trans_dir[..., None] * scaled[:, :, None, :]
    own_read = jnp.einsum("bhvk,bhk->bhv", state, query_t, precision=lax.Precision.HIGHEST)
    trans_read = jnp.einsum("bhjk,bhk->bhj", trans, query_t, precision=lax.Precision.HIGHEST)
    return ((state, trans), (own_read, trans_read))


def per_device(
    resid,
    queries,
    keys,
    values,
    decay_input_part,
    decay_channel_offset,
    decay_head_extra,
    correction_rate_input,
    correction_rate_offset,
    head_norm_gain,
    mixer_output_weight,
    feedforward_norm_gain,
    gate_weight,
    up_weight,
    down_weight,
):
    tok_rows = queries.shape[0]
    local_heads = queries.shape[1] // HEAD
    blocks = tok_rows // BLK

    def head_count(arr):
        return arr.astype(jnp.float32).reshape(tok_rows, local_heads, HEAD)

    def to_steps(arr):
        return jnp.moveaxis(arr.reshape(blocks, BLK, local_heads, HEAD), 1, 0)

    correction_rate = jnp.exp(
        -jax.nn.softplus(-(decay_channel_offset + decay_input_part.astype(jnp.float32))) - 0.5
    )
    decay_factor = jnp.exp(-head_count(correction_rate) - decay_head_extra[:, :, None])
    key_f = head_count(keys)
    unit_keys = key_f * lax.rsqrt(jnp.sum(key_f * key_f, axis=-1, keepdims=True) + 1e-06)
    lrate = head_count(
        jax.nn.sigmoid(correction_rate_offset + correction_rate_input.astype(jnp.float32))
    )
    identity = jnp.broadcast_to(jnp.eye(HEAD, dtype=jnp.float32), (local_heads, HEAD, HEAD))
    zeros = jnp.zeros((local_heads, HEAD, HEAD), jnp.float32)
    start = (
        jnp.zeros((blocks, local_heads, HEAD, HEAD), jnp.float32),
        jnp.broadcast_to(identity, (blocks, local_heads, HEAD, HEAD)),
    )
    step_inputs = tuple(
        (
            to_steps(arr)
            for arr in (
                head_count(queries),
                decay_factor,
                key_f,
                head_count(values),
                unit_keys,
                lrate,
            )
        )
    )
    (end_state, end_trans), (own_read, trans_read) = lax.scan(block_step, start, step_inputs)
    inclusive = lax.associative_scan(combine, (end_trans, end_state), axis=0)
    device_total = (inclusive[0][-1], inclusive[1][-1])
    prefix_trans = jnp.concatenate([identity[None], inclusive[0][:-1]], axis=0)
    prefix_state = jnp.concatenate([zeros[None], inclusive[1][:-1]], axis=0)
    _, incoming = entering(device_total, SP, combine, (identity, zeros))
    block_start = (
        jnp.einsum("hvk,bhkj->bhvj", incoming, prefix_trans, precision=lax.Precision.HIGHEST)
        + prefix_state
    )
    reads = (
        jnp.einsum("bhvk,tbhk->tbhv", block_start, trans_read, precision=lax.Precision.HIGHEST)
        + own_read
    )
    mixer_out = jnp.moveaxis(reads, 0, 1).reshape(tok_rows, local_heads, HEAD)
    center = mixer_out - jnp.mean(mixer_out, axis=-1, keepdims=True)
    spread = jnp.mean(center * center, axis=-1, keepdims=True)
    mixed = (
        (center * lax.rsqrt(spread + 1e-05) * head_norm_gain.reshape(local_heads, HEAD))
        .reshape(tok_rows, -1)
        .astype(jnp.bfloat16)
    )
    row_mixed = lax.all_to_all(mixed, "tp", split_axis=0, concat_axis=1, tiled=True)
    proj = jnp.dot(row_mixed, mixer_output_weight, preferred_element_type=jnp.float32)
    mid_f = (resid.astype(jnp.float32) + proj).astype(jnp.bfloat16).astype(jnp.float32)
    normed = (
        mid_f
        * lax.rsqrt(jnp.mean(mid_f * mid_f, axis=-1, keepdims=True) + 1e-06)
        * feedforward_norm_gain
    ).astype(jnp.bfloat16)
    whole_rows = gathered_copies(normed, "tp", 0)
    pieces = sent_together((gate_weight, up_weight), SP, 0, 1)
    gate = jnp.dot(whole_rows, pieces[0], preferred_element_type=jnp.float32)
    upper = jnp.dot(whole_rows, pieces[1], preferred_element_type=jnp.float32)
    whole_down = whole_of(down_weight, SP, 1)
    hidden = (jax.nn.silu(gate) * upper).astype(jnp.bfloat16)
    down_sum = sent_and_summed(
        jnp.dot(hidden, whole_down, preferred_element_type=jnp.float32).astype(jnp.bfloat16),
        "tp",
        0,
    )
    return (mid_f + 0.5 * down_sum).astype(jnp.bfloat16)


def solution(mesh):
    torus = Mesh(mesh.devices.reshape(8, 4, mesh.shape["tp"]), ("sp_0", "sp_1", "tp"))
    in_specs = (
        P(SP_TP, None),
        P(SP, "tp"),
        P(SP, "tp"),
        P(SP, "tp"),
        P(SP, "tp"),
        P("tp"),
        P(SP, "tp"),
        P(SP, "tp"),
        P("tp"),
        P("tp"),
        P(),
        P(),
        P(SP, "tp"),
        P(SP, "tp"),
        P("tp", SP),
    )
    out_specs = P(SP_TP, None)
    return jax.shard_map(
        per_device, mesh=torus, in_specs=in_specs, out_specs=out_specs, check_vma=False
    )
```

profile of v0, /device:TPU:1, one launch (start us, length us, event | category | flops | bytes accessed | tf_op | source)
XLA Modules:
  0.0 570.8 jit_solution(1547033450938407414)
XLA Ops:
  8.4 12.8 %all_gather.26 = bf16[704,256]{0,1:T(8,128)(2,1)} all-gather(bf16[704,64]{0,1:T(8,128)(2,1)} %param.31), channel_id=1, replica_groups=mesh['sp_0'=8,'sp_1'=4,'tp'=8] {'sp_1'}, dimensions={1}, use_global_device_ids=true | all-gather | bytes 450560 | tf_op jit(solution)/shard_map/all_gather | solution.py:87
  27.4 2.6 multiply_bitcast_fusion
  30.2 291.0 %while.17 = (s32[]{:T(128)}, f32[24,2,64,64]{3,2,1,0:T(8,128)S(1)}, f32[24,2,64,64]{3,2,1,0:T(8,128)S(1)}, f32[16,24,2,64]{3,0,2,1:T(8,128)}, f32[16,24,2,64]{3,...) while((s32[]{:T(128)}, f32[24,2,64,64]{3,2,1,0:T(8,128)S(1)}, ...), condition=%wide.region_2.3_spmd.clone, body=%wide.region_1.2_spmd.clone.sunk | while | flops 11409411 | bytes 6660256 | solution.py:183
  327.0 3.4 pad.59
  333.9 4.3 pad.62
  341.2 4.3 pad.61
  349.7 7.2 %pad.64 = f32[12,2,64,64]{3,2,1,0:T(8,128)} pad(f32[6,2,64,64]{3,2,1,0:T(8,128)} %copy-done.4, f32[]{:T(128)} %constant.26.clone.1), padding=1_0_1x0_0_0x0_0_0x0_0_0 | pad | bytes 589828 | tf_op jit(solution)/shard_map/pad | solution.py:184
  359.3 7.2 %pad.63 = f32[12,2,64,64]{3,2,1,0:T(8,128)} pad(f32[6,2,64,64]{3,2,1,0:T(8,128)} %pad_maximum_fusion.3, f32[]{:T(128)} %constant.26.clone.1), padding=0_1_1x0_0_0x0_0_0x0_0_0 | pad | bytes 589828 | tf_op jit(solution)/shard_map/pad | solution.py:184
  370.6 12.9 %pad.66 = f32[24,2,64,64]{3,2,1,0:T(8,128)} pad(f32[12,2,64,64]{3,2,1,0:T(8,128)} %copy-done.5, f32[]{:T(128)} %constant.26.clone.1), padding=1_0_1x0_0_0x0_0_0x0_0_0 | pad | bytes 1179652 | tf_op jit(solution)/shard_map/pad | solution.py:184
  385.8 2.6 pad.53
  390.0 4.6 pad.56
  395.3 4.6 pad.55
  404.0 8.6 %pad.65 = f32[24,2,64,64]{3,2,1,0:T(8,128)} pad(f32[12,2,64,64]{3,2,1,0:T(8,128)S(1)} %pad_maximum_fusion.1, f32[]{:T(128)} %constant.26.clone.1), padding=0_1_1x0_0_0x0_0_0x0_0_0 | pad | bytes 1179652 | tf_op jit(solution)/shard_map/pad | solution.py:184
  413.4 9.9 %all-gather = bf16[1024,64]{1,0:T(8,128)(2,1)S(1)} all-gather(bf16[256,64]{1,0:T(8,128)(2,1)S(1)} %pad_maximum_fusion.9), channel_id=2, replica_groups=mesh['sp_0'=8,'sp_1'=4,'tp'=8] {'sp_1'}, dimensions={0}, use_global_device_ids=true | all-gather | bytes 163840 | tf_op jit(solution)/shard_map/all_gather | solution.py:27
  424.7 22.4 %all-gather.1 = bf16[2048,64]{1,0:T(8,128)(2,1)S(1)} all-gather(bf16[256,64]{1,0:T(8,128)(2,1)S(1)} %pad_maximum_fusion.10), channel_id=3, replica_groups=mesh['sp_0'=8,'sp_1'=4,'tp'=8] {'sp_0'}, dimensions={0}, use_global_device_ids=true | all-gather | bytes 294912 | tf_op jit(solution)/shard_map/all_gather | solution.py:27
  451.1 8.8 %pad.93 = f32[23,2,64,64]{3,2,1,0:T(8,128)} pad(f32[12,2,64,64]{3,2,1,0:T(8,128)S(1)} %pad_maximum_fusion.1, f32[]{:T(128)} %constant.26.clone.1), padding=0_0_1x0_0_0x0_0_0x0_0_0 | pad | bytes 1146884 | tf_op jit(solution)/shard_map/slice | solution.py:187
  460.1 9.3 %pad.57 = f32[24,2,64,64]{3,2,1,0:T(8,128)S(1)} pad(f32[12,2,64,64]{3,2,1,0:T(8,128)} %pad_maximum_fusion, f32[]{:T(128)} %constant.26.clone.1), padding=0_1_1x0_0_0x0_0_0x0_0_0 | pad | bytes 1179652 | tf_op jit(solution)/shard_map/pad | solution.py:184
  472.7 2.6 fusion.105
  478.3 21.4 %all_to_all.26 = bf16[8,48,128]{2,1,0:T(8,128)(2,1)S(1)} all-to-all(bf16[8,48,128]{2,1,0:T(8,128)(2,1)S(1)} %multiply_convert_fusion.1), channel_id=1, replica_groups=mesh['sp_0'=8,'sp_1'=4,'tp'=8] {'tp'}, dimensions={0} | all-to-all | bytes 196608 | tf_op jit(solution)/shard_map/all_to_all | solution.py:205
  499.7 3.2 multiply_reduce_fusion
  503.2 23.8 %all_to_all.27 = bf16[8,48,2048]{2,1,0:T(8,128)(2,1)S(1)} all-to-all(bf16[8,48,2048]{2,1,0:T(8,128)(2,1)S(1)} %broadcast_in_dim.44), channel_id=1, replica_groups=mesh['sp_0'=8,'sp_1'=4,'tp'=8] {'tp'}, dimensions={0} | all-to-all | bytes 3145728 | tf_op jit(solution)/shard_map/all_to_all | solution.py:68
  527.0 4.6 fusion.8
  531.5 7.4 %convolution_convert_fusion = bf16[384,2048]{1,0:T(8,128)(2,1)S(1)} fusion(bf16[704,2048]{0,1:T(8,128)(2,1)} %all-gather.7.cloned.1.call-done, bf16[384,2048]{1,0:T(8,128)(2,1)S(1)} %bitcast.255, bf16[2048,1408]{1,0:T(8,128)(2,1)} %all-gather.5.cloned.1.call-done, f32[384,704]{0,1:T(8,128)} %fusion.8), kind=kOutput, calls=%fused_computation.21 | convolution fusion | flops 2217000960 | bytes 10518528 | tf_op jit(solution)/shard_map/dot_general | solution.py:220
  538.9 24.0 %all_to_all.28 = bf16[8,48,2048]{2,1,0:T(8,128)(2,1)S(1)} all-to-all(bf16[8,48,2048]{2,1,0:T(8,128)(2,1)S(1)} %bitcast.256), channel_id=1, replica_groups=mesh['sp_0'=8,'sp_1'=4,'tp'=8] {'tp'}, dimensions={0} | all-to-all | bytes 3145728 | tf_op jit(solution)/shard_map/all_to_all | solution.py:98
  (378 shorter events, 343.5 us)
Async XLA Ops:
  6.5 17.1 %copy-start.33 = (bf16[384,128]{1,0:T(8,128)(2,1)S(1)}, bf16[384,128]{1,0:T(8,128)(2,1)}, u32[]{:S(2)}) copy-start(bf16[384,128]{1,0:T(8,128)(2,1)} %param.21) | copy-start | bytes 294916
  6.5 17.1 %copy-start.39 = (f32[128]{0:T(128)S(1)}, f32[128]{0:T(128)}, u32[]{:S(2)}) copy-start(f32[128]{0:T(128)} %param.22) | copy-start | bytes 1540
  6.5 520.4 %all-gather.5.cloned.1.call-start = ((), (), s32[]{:S(2)}) async-start(), calls=%async_computation.3 | async-start | bytes 5947392 | tf_op jit(solution)/shard_map/all_gather | solution.py:77
  8.3 15.8 %copy-start.38 = (f32[384,2]{0,1:T(2,128)S(1)}, f32[384,2]{0,1:T(2,128)}, u32[]{:S(2)}) copy-start(f32[384,2]{0,1:T(2,128)} %param.23) | copy-start | bytes 9220
  8.3 523.2 %all-gather.7.cloned.1.call-start = ((), (), s32[]{:S(2)}) async-start(), calls=%async_computation.4 | async-start | bytes 3538944 | tf_op jit(solution)/shard_map/all_gather | solution.py:87
  21.2 3.1 copy-start.34
  21.2 3.1 copy-start.40
  22.3 3.1 copy-start.35
  22.5 7.6 %copy-start.11 = (f32[64,64]{1,0:T(8,128)}, f32[64,64]{1,0:T(8,128)S(1)}, u32[]{:S(2)}) copy-start(f32[64,64]{1,0:T(8,128)S(1)} %fusion.84) | copy-start | bytes 49156
  22.5 3.9 copy-start.36
  370.6 12.9 %copy-start.9 = (f32[3,2,64,64]{3,2,1,0:T(8,128)S(1)}, f32[3,2,64,64]{3,2,1,0:T(8,128)}, u32[]{:S(2)}) copy-start(f32[3,2,64,64]{3,2,1,0:T(8,128)} %copy-done.8) | copy-start | bytes 294916
  370.6 13.9 %slice-start.1 = ((f32[3,2,64,64]{3,2,1,0:T(8,128)}), f32[1,2,64,64]{3,2,1,0:T(8,128)S(1)}, s32[]{:S(2)}) async-start(f32[3,2,64,64]{3,2,1,0:T(8,128)} %copy-done.8), calls=%async_computation.6 | async-start | bytes 131072 | tf_op jit(solution)/shard_map/slice | solution.py:184
  384.6 4.9 copy-start.1
  388.5 6.8 %slice-start = ((f32[12,2,64,64]{3,2,1,0:T(8,128)}), f32[1,2,64,64]{3,2,1,0:T(8,128)S(1)}, s32[]{:S(2)}) async-start(f32[12,2,64,64]{3,2,1,0:T(8,128)} %copy-done), calls=%async_computation.5 | async-start | bytes 131072 | tf_op jit(solution)/shard_map/slice | solution.py:184
  394.6 5.3 copy-start.7
  404.0 19.4 %copy-start.12 = (f32[64,64]{1,0:T(8,128)S(1)}, f32[64,64]{1,0:T(8,128)}, u32[]{:S(2)}) copy-start(f32[64,64]{1,0:T(8,128)} %copy-done.11) | copy-start | bytes 49156
  423.5 24.5 %copy-start.17 = (f32[1,2,64,64]{3,2,1,0:T(8,128)S(1)}, f32[1,2,64,64]{3,2,1,0:T(8,128)}, u32[]{:S(2)}) copy-start(f32[1,2,64,64]{3,2,1,0:T(8,128)} %slice.260) | copy-start | bytes 98308
  448.0 2.0 copy-start.21
  448.0 2.0 copy-start.22
  448.0 2.1 copy-start.20
  469.7 1.9 copy-start.3
  476.4 1.9 copy-start.41
  477.0 22.6 %copy-start.19 = (bf16[48,2048]{1,0:T(8,128)(2,1)S(1)}, bf16[48,2048]{1,0:T(8,128)(2,1)}, u32[]{:S(2)}) copy-start(bf16[48,2048]{1,0:T(8,128)(2,1)} %param.17) | copy-start | bytes 589828
  499.7 3.2 copy-start.37
  (22 other events, 28.5 us)
Sparse Core Ops, SparseCore 0:
  9.9 88.5 all-gather.4
  100.3 42.9 all-gather.6
where the time goes:
time: 581 us; the launch traced here: 571 us
  matrix products  197 us (34%)
  local copies, waits for them, and re-layouts  187 us (32%)
  blocking collectives  114 us (20%)
  other arithmetic  58 us (10%)
  between operations  14.5 us (2%)
    pad x14, local copies, waits for them, and re-layouts, per_device(): inclusive = lax.associative_scan(combine, (end_trans, end_state), axis=0)  69.4 us
    dynamic_update_slice x32, local copies, waits for them, and re-layouts, per_device(): lax.scan(block_step, start, step_inputs)  54.3 us
    dot_general x16, matrix products, block_step(): jnp.einsum('bhjk,bhk->bhj', trans, lifted, precision=lax.Precision.HIGHEST)  40.9 us
    dot_general x16, matrix products, block_step(): jnp.einsum('bhvk,bhk->bhv', state, lifted, precision=lax.Precision.HIGHEST)  40.8 us
    dot_general x16, matrix products, block_step(): jnp.einsum('bhjk,bhk->bhj', trans, query_t, precision=lax.Precision.HIGHEST)  40.6 us
    dot_general x16, matrix products, block_step(): jnp.einsum('bhvk,bhk->bhv', state, query_t, precision=lax.Precision.HIGHEST)  40.6 us
    all_gather x2, blocking collectives, gathered_once(): both, at, found = (lax.all_gather(jnp.concatenate(lines), axis), 0, {})  32.3 us
    add x16, other arithmetic, block_step(): trans * decay_t[:, :, None, :]  24.8 us
  transfers between devices with their start and end apart: 2, of which 0 were waited for; matrix products, arithmetic and copies ran while one was open for 75% of the time, Pallas kernels for 0%

commit v1 on v0

v1 whole, which is shorter than its diff:
```python
import jax
import jax.numpy as jnp
from jax import lax
from jax.experimental import pallas as pl
from jax.experimental.pallas import tpu as pltpu
from jax.sharding import Mesh
from jax.sharding import PartitionSpec as P

HEAD = 64
C = 64
SP = ("sp_0", "sp_1")
SP_TP = ("sp_0", "sp_1", "tp")
BF = jnp.bfloat16
F32 = jnp.float32


def split(x):
    hi = x.astype(BF)
    return hi, (x - hi.astype(F32)).astype(BF)


def dot(a, b):
    return lax.dot_general(a, b, (((1,), (0,)), ((), ())), preferred_element_type=F32)


def dot_t(a, b):
    return lax.dot_general(a, b, (((1,), (1,)), ((), ())), preferred_element_type=F32)


def mm(x, y, f=dot):
    return f(x[0], y[0]) + (f(x[0], y[1]) + f(x[1], y[0]))


def iota(shape, dim):
    return lax.broadcasted_iota(jnp.int32, shape, dim)


def head_masks(width=128):
    first = (iota((1, width), 1) & 127) < HEAD
    m0 = jnp.where(first, 1.0, 0.0)
    return m0.astype(BF), (1.0 - m0).astype(BF)


def stacked(y, masks):
    return tuple(jnp.concatenate([p * masks[0], p * masks[1]], axis=0) for p in y)


def local_scan(q, k, v, dx, lx, dco, lro, extra):
    tok = q.shape[0]
    first = iota((1, 128), 1) < HEAD
    masks, masks2 = head_masks(), head_masks(256)
    ext = jnp.where(first, extra[:, 0:1], extra[:, 1:2])
    log_decay = -0.6065306597126334 * (1.0 / (1.0 + jnp.exp(-(dco + dx)))) - ext
    lrate = 1.0 / (1.0 + jnp.exp(-(lro + lx)))
    same = (iota((128, 128), 0) < HEAD) == (iota((128, 128), 1) < HEAD)
    same_f = jnp.where(same, 1.0, 0.0)
    ones = same_f.astype(BF)
    kk = split(k * k)
    unit = k * lax.rsqrt(dot(kk[0], ones) + dot(kk[1], ones) + 1e-06)
    rate = lrate * unit
    row, col = iota((C, 128), 0), iota((C, 128), 1) & (C - 1)
    lower = row > col
    lower_eq = row >= col
    eye_packed = jnp.where(row == col, 1.0, 0.0)
    tri = jnp.where(iota((C, C), 0) >= iota((C, C), 1), 1.0, 0.0).astype(BF)
    eye = jnp.where(iota((128, 128), 0) == iota((128, 128), 1), 1.0, 0.0)
    levels = [
        ((row >> n) == (col >> n) + 1) & (((row >> n) & 1) == 1) for n in range(6)
    ]
    steps = []
    for c in range(tok // C):
        at = slice(c * C, (c + 1) * C)
        lw = log_decay[at]
        w0 = lw.astype(BF)
        w1, w2 = split(lw - w0.astype(F32))
        cum = dot(tri, w0) + (dot(tri, w1) + dot(tri, w2))
        mid, end = cum[C // 2 - 1 : C // 2], cum[C - 1 : C]
        grow = jnp.exp(cum - mid)
        fall = jnp.exp(mid - cum)
        pc = jnp.exp(cum - lw - mid) * unit[at]
        uc = grow * q[at]
        rc = fall * rate[at]
        gc = fall * k[at]
        left = split(jnp.concatenate([pc, uc], axis=0))
        rs, gs = stacked(split(rc), masks), stacked(split(gc), masks)
        right = tuple(jnp.concatenate([a, b], axis=0) for a, b in zip(rs, gs))
        pair = mm(left, right, dot_t)
        arp = jnp.where(lower, pair[:C, :128], 0.0)
        agp = jnp.where(lower, pair[:C, 128:], 0.0)
        bur = jnp.where(lower_eq, pair[C:, :128], 0.0)
        bug = jnp.where(lower_eq, pair[C:, 128:], 0.0)
        vs = stacked((v[at].astype(BF),), masks)[0]
        ab = split(jnp.concatenate([agp, bug], axis=0))
        abv = dot(ab[0], vs) + dot(ab[1], vs)
        inv = eye_packed - jnp.where(levels[0], arp, 0.0)
        for n in range(1, 6):
            s = split(inv)
            t = mm(split(jnp.where(levels[n], arp, 0.0)), stacked(s, masks))
            inv = inv - mm(s, stacked(split(t), masks))
        to_mid = jnp.exp(mid)
        rest = jnp.exp(end - mid)
        pt = jnp.concatenate([pc * to_mid, abv[:C]], axis=1)
        wy = mm(split(inv), stacked(split(pt), masks2))
        wys = split(wy)
        bwy = mm(split(bur), stacked(wys, masks2))
        ueff = uc * to_mid - bwy[:, :128]
        own = abv[C:] - bwy[:, 128:]
        r_end = (rc * rest).T
        g_end = (gc * rest).T
        rs_t = split(r_end)
        rwy = mm(rs_t, wys)
        gs_t = split(g_end)
        vb = v[at].astype(BF)
        gv = dot(gs_t[0], vb) + dot(gs_t[1], vb)
        trans = eye * jnp.exp(end) - same_f * rwy[:, :128]
        state = same_f * (gv - rwy[:, 128:])
        steps.append((ueff, own, trans, state))
    reads, owns = [], []
    both = jnp.concatenate([eye, jnp.zeros((128, 128), F32)], axis=1)
    for ueff, own, trans, state in steps:
        bs = split(both)
        out = mm(split(ueff), bs)
        reads.append(out[:, :128])
        owns.append(own + out[:, 128:])
        both = mm(split(trans), bs)
        both = jnp.concatenate([both[:, :128], both[:, 128:] + state], axis=1)
    total = jnp.concatenate(
        [both[:HEAD, :128] + both[HEAD:, :128], both[:HEAD, 128:] + both[HEAD:, 128:]], axis=0
    )
    return jnp.concatenate(reads, axis=0), jnp.concatenate(owns, axis=0), total


def local_kernel(q, k, v, dx, lx, dco, lro, extra, reads, owns, total):
    f = lambda r: r[...].astype(F32)
    a, b, t = local_scan(f(q), f(k), f(v), f(dx), f(lx), dco[...], lro[...], extra[...])
    reads[...] = a
    owns[...] = b
    total[...] = t.astype(BF)


def finish(reads, owns, state, gain):
    masks = head_masks()
    out = owns + mm(split(reads), stacked(split(state), masks))
    same = (iota((128, 128), 0) < HEAD) == (iota((128, 128), 1) < HEAD)
    mean = jnp.where(same, 1.0 / HEAD, 0.0).astype(BF)
    s = split(out)
    center = out - (dot(s[0], mean) + dot(s[1], mean))
    s = split(center * center)
    spread = dot(s[0], mean) + dot(s[1], mean)
    return (center * lax.rsqrt(spread + 1e-05) * gain).astype(BF)

def fold(level, masks2, exact):
    while len(level) > 1:
        nxt = []
        for i in range(0, len(level) - 1, 2):
            (t1, x1), (t2, x2) = level[i], level[i + 1]
            both = jnp.concatenate([t1, x1], axis=1)
            if exact:
                out = dot(t2.astype(BF), stacked((both.astype(BF),), masks2)[0])
            else:
                out = mm(split(t2), stacked(split(both), masks2))
            nxt.append((out[:, :128], out[:, 128:] + x2))
        if len(level) % 2:
            nxt.append(level[-1])
        level, exact = nxt, False
    return level[0]


def piece(pieces, d):
    p = pieces[d].astype(F32)
    return p[:HEAD], p[HEAD:]


def earlier(pieces, count, index, masks2):
    eye_packed = jnp.where(iota((HEAD, 128), 0) == (iota((HEAD, 128), 1) & (HEAD - 1)), 1.0, 0.0)
    level = []
    for d in range(count - 1):
        used = jnp.where(d < index, 1.0, 0.0)
        trans, state = piece(pieces, d)
        level.append((trans * used + eye_packed * (1.0 - used), state * used))
    return fold(level, masks2, True)


def group_kernel(index, pieces, total, inside):
    masks2 = head_masks(256)
    count = pieces.shape[0]
    t, x = fold([piece(pieces, d) for d in range(count)], masks2, True)
    total[...] = jnp.concatenate([t, x], axis=0).astype(BF)
    t, x = earlier(pieces, count, index[0], masks2)
    inside[...] = jnp.concatenate([t, x], axis=0)


def finish_kernel(index, pieces, inside, reads, owns, gain, mixed):
    _, x = earlier(pieces, pieces.shape[0], index[0], head_masks(256))
    t = inside[...]
    state = mm(split(t[:HEAD]), stacked(split(x), head_masks())) + t[HEAD:]
    mixed[...] = finish(reads[...], owns[...], state, gain[...])


def vmem(n):
    return [pl.BlockSpec(memory_space=pltpu.VMEM)] * n


SMEM = pl.BlockSpec(memory_space=pltpu.SMEM)


def from_everyone(array, axis):
    copies = jnp.broadcast_to(array, (lax.axis_size(axis), *array.shape))
    return lax.all_to_all(copies, axis, split_axis=0, concat_axis=0, tiled=True)


def per_device(
    resid,
    queries,
    keys,
    values,
    decay_input_part,
    decay_channel_offset,
    decay_head_extra,
    correction_rate_input,
    correction_rate_offset,
    head_norm_gain,
    mixer_output_weight,
    feedforward_norm_gain,
    gate_weight,
    up_weight,
    down_weight,
):
    tok = queries.shape[0]
    shape = jax.ShapeDtypeStruct
    cols = gate_weight.shape[1]
    weights = lax.all_gather(
        jnp.concatenate([gate_weight, up_weight, down_weight.T], axis=1), SP, axis=0, tiled=True
    )
    reads, owns, total = pl.pallas_call(
        local_kernel,
        out_shape=(shape((tok, 128), F32), shape((tok, 128), F32), shape((128, 128), BF)),
        in_specs=vmem(8),
        out_specs=tuple(vmem(3)),
        name="local",
    )(
        queries,
        keys,
        values,
        decay_input_part,
        correction_rate_input,
        decay_channel_offset[None],
        correction_rate_offset[None],
        decay_head_extra,
    )
    near = from_everyone(total, "sp_1")
    total, inside = pl.pallas_call(
        group_kernel,
        out_shape=(shape((128, 128), BF), shape((128, 128), F32)),
        in_specs=[SMEM] + vmem(1),
        out_specs=tuple(vmem(2)),
        name="group",
    )(lax.axis_index("sp_1")[None], near)
    far = from_everyone(total, "sp_0")
    mixed = pl.pallas_call(
        finish_kernel,
        out_shape=shape((tok, 128), BF),
        in_specs=[SMEM] + vmem(5),
        out_specs=vmem(1)[0],
        name="finish",
    )(lax.axis_index("sp_0")[None], far, inside, reads, owns, head_norm_gain[None])
    row_mixed = lax.all_to_all(mixed, "tp", split_axis=0, concat_axis=1, tiled=True)
    proj = jnp.dot(row_mixed, mixer_output_weight, preferred_element_type=F32)
    mid_f = (resid.astype(F32) + proj).astype(BF).astype(F32)
    normed = (
        mid_f
        * lax.rsqrt(jnp.mean(mid_f * mid_f, axis=-1, keepdims=True) + 1e-06)
        * feedforward_norm_gain
    ).astype(BF)
    rows = from_everyone(normed, "tp").reshape(tok, -1)
    both = jnp.dot(rows, weights[:, : 2 * cols], preferred_element_type=F32)
    hidden = (jax.nn.silu(both[:, :cols]) * both[:, cols:]).astype(BF)
    partial = lax.dot_general(
        hidden, weights[:, 2 * cols :], (((1,), (1,)), ((), ())), preferred_element_type=F32
    ).astype(BF)
    pieces = lax.all_to_all(
        partial.reshape(8, -1, partial.shape[1]), "tp", 0, 0, tiled=True
    )
    down_sum = jnp.sum(pieces.astype(F32), axis=0)
    return (mid_f + 0.5 * down_sum).astype(BF)


def solution(mesh):
    torus = Mesh(mesh.devices.reshape(8, 4, mesh.shape["tp"]), ("sp_0", "sp_1", "tp"))
    in_specs = (
        P(SP_TP, None),
        P(SP, "tp"),
        P(SP, "tp"),
        P(SP, "tp"),
        P(SP, "tp"),
        P("tp"),
        P(SP, "tp"),
        P(SP, "tp"),
        P("tp"),
        P("tp"),
        P(),
        P(),
        P(SP, "tp"),
        P(SP, "tp"),
        P("tp", SP),
    )
    return jax.shard_map(
        per_device, mesh=torus, in_specs=in_specs, out_specs=P(SP_TP, None), check_vma=False
    )
```

time: 581 us -> 158 us (0.27); the launches traced: 571 us -> 157 us
  matrix products: 197 us -> 11.8 us
  local copies, waits for them, and re-layouts: 187 us -> 7.86 us
  other arithmetic: 58 us -> 1.07 us
  blocking collectives: 114 us -> 62.9 us
  waiting for transfers between devices: 0.04 us -> 24 us
  Pallas kernels: 0 us -> 22.8 us
  starting transfers between devices: 0.04 us -> 13.1 us
    dot_general x104 -> x3, matrix products: 197 us -> 11.8 us  [the longest x1 5.22 us: per_device(): both = jnp.dot(rows, weights[:, :2 * cols], preferred_element_type=F32)]
    pad x14 -> x0, local copies, waits for them, and re-layouts: 69.4 us -> none  [per_device(): inclusive = lax.associative_scan(combine, (end_trans, end_state), axis=0)]
    dynamic_update_slice x32 -> x0, local copies, waits for them, and re-layouts: 54.3 us -> none  [per_device(): lax.scan(block_step, start, step_inputs)]
    all_gather x3 -> x0, blocking collectives: 45.1 us -> none  [the longest x2 32.3 us: gathered_once(): both, at, found = (lax.all_gather(jnp.concatenate(lines), axis), 0, {})]
    add x24 -> x0, other arithmetic: 31.3 us -> none  [the longest x16 24.8 us: block_step(): trans * decay_t[:, :, None, :]]
    mul x34 -> x0, local copies, waits for them, and re-layouts: 24.9 us -> none  [the longest x16 12.3 us: block_step(): value_t[..., None] * key_t[:, :, None, :]]
    pallas_call x0 -> x3, Pallas kernels: none -> 22.8 us  [the longest x1 17.9 us: per_device(): pl.pallas_call(local_kernel, out_shape=(shape((tok, 128), F32), shape((to...]
    all_to_all x0 -> x2, waiting for transfers between devices: none -> 14.2 us  [from_everyone(): return lax.all_to_all(copies, axis, split_axis=0, concat_axis=0, tiled=True)]
  transfers between devices with their start and end apart: 2 -> 3, of which waited for: 0 -> 3; matrix products, arithmetic and copies ran while one was open for 75% -> 5% of each run, Pallas kernels for 0% -> 15%
where the time goes in v1:
time: 158 us; the launch traced here: 157 us
  blocking collectives  62.9 us (40%)
  waiting for transfers between devices  24 us (15%)
  Pallas kernels  22.8 us (14%)
  between operations  13.5 us (9%)
  starting transfers between devices  13.1 us (8%)
  matrix products  11.8 us (7%)
  local copies, waits for them, and re-layouts  7.86 us (5%)
    all_to_all x1, blocking collectives, per_device(): lax.all_to_all(partial.reshape(8, -1, partial.shape[1]), 'tp', 0, 0, tile...  26 us
    all_to_all x1, blocking collectives, from_everyone(): return lax.all_to_all(copies, axis, split_axis=0, concat_axis=0, tiled=True)  23.8 us
    pallas_call x1, Pallas kernels, per_device(): pl.pallas_call(local_kernel, out_shape=(shape((tok, 128), F32), shape((to...  17.9 us
    all_to_all x2, waiting for transfers between devices, from_everyone(): return lax.all_to_all(copies, axis, split_axis=0, concat_axis=0, tiled=True)  14.2 us
    all_to_all x2, starting transfers between devices, from_everyone(): return lax.all_to_all(copies, axis, split_axis=0, concat_axis=0, tiled=True)  13.1 us
    all_to_all x1, blocking collectives, per_device(): lax.all_to_all(mixed, 'tp', split_axis=0, concat_axis=1, tiled=True)  13.1 us
    all_gather x1, waiting for transfers between devices, per_device(): lax.all_gather(jnp.concatenate([gate_weight, up_weight, down_weight.T], a...  9.86 us
    dot_general x1, matrix products, per_device(): both = jnp.dot(rows, weights[:, :2 * cols], preferred_element_type=F32)  5.22 us
  transfers between devices with their start and end apart: 3, of which 3 were waited for; matrix products, arithmetic and copies ran while one was open for 5% of the time, Pallas kernels for 15%

profile of v1, /device:TPU:1, one launch (start us, length us, event | category | flops | bytes accessed | tf_op | source)
XLA Modules:
  0.0 157.1 jit_solution(566151795254462547)
XLA Ops:
  6.5 1.9 %concatenate.3 = bf16[64,2112]{1,0:T(8,128)(2,1)} concatenate(bf16[64,704]{1,0:T(8,128)(2,1)} %param.27, bf16[64,704]{1,0:T(8,128)(2,1)} %param.28, bf16[64,704]{1,0:T(8,128)(2,1)} %bitcast.24), dimensions={1} | concatenate | bytes 540672 | tf_op jit(solution)/shard_map/concatenate | solution.py:233
  8.5 1.5 copy.19.extra
  10.0 17.9 %local.1 = (f32[384,128]{1,0:T(8,128)}, f32[384,128]{1,0:T(8,128)}, bf16[128,128]{1,0:T(8,128)(2,1)}) custom-call(bf16[384,128]{1,0:T(8,128)(2,1)} %q.1, bf16[384,128]{1,0:T(8,128)(2,1)} %k.1, bf16[384,128]{1,0:T(8,128)(2,1)} %v.1, bf16[384,128]{1,0:T(8,128)(2,1)} %dx.1, bf16[384,128]{1,0:T(8,128)(2,1)} %lx.1, f32[1,128]{1,0:T(1,128)} %bitcast.26, ...), custom_call_target="tpu_custom_call" | custom-call | tf_op jit(solution)/shard_map/local/pallas_call | solution.py:235
  27.8 1.4 broadcast_in_dim.30
  29.2 4.8 %all-to-all-start = ((bf16[4,128,128]{2,1,0:T(8,128)(2,1)}), bf16[4,128,128]{2,1,0:T(8,128)(2,1)S(1)}, u32[]{:S(2)}, u32[]{:S(2)}) async-start(bf16[4,128,128]{2,1,0:T(8,128)(2,1)} %broadcast_in_dim.30), calls=%async_computation | async-start | bytes 262144 | tf_op jit(solution)/shard_map/all_to_all | solution.py:209
  34.1 4.8 %all-to-all-done.pieces = bf16[4,128,128]{2,1,0:T(8,128)(2,1)S(1)} async-done(((bf16[4,128,128]{2,1,0:T(8,128)(2,1)}), bf16[4,128,128]{2,1,0:T(8,128)(2,1)S(1)}, u32[]{:S(2)}, u32[]{:S(2)}) %all-to-all-start) | async-done | bytes 131104 | tf_op jit(solution)/shard_map/all_to_all | solution.py:209
  38.9 0.7 copy-done.1
  39.6 1.9 %group.1 = (bf16[128,128]{1,0:T(8,128)(2,1)}, f32[128,128]{1,0:T(8,128)}) custom-call(s32[1]{0:T(128)} %bitcast.1.index, bf16[4,128,128]{2,1,0:T(8,128)(2,1)} %copy-done.1), custom_call_target="tpu_custom_call" | custom-call | tf_op jit(solution)/shard_map/group/pallas_call | solution.py:252
  41.5 1.5 broadcast_in_dim.31
  42.9 8.3 %all-to-all-start.1 = ((bf16[8,128,128]{2,1,0:T(8,128)(2,1)}), bf16[8,128,128]{2,1,0:T(8,128)(2,1)S(1)}, u32[]{:S(2)}, u32[]{:S(2)}) async-start(bf16[8,128,128]{2,1,0:T(8,128)(2,1)} %broadcast_in_dim.31), calls=%async_computation.1 | async-start | bytes 524288 | tf_op jit(solution)/shard_map/all_to_all | solution.py:209
  51.3 9.3 %all-to-all-done.1.pieces = bf16[8,128,128]{2,1,0:T(8,128)(2,1)S(1)} async-done(((bf16[8,128,128]{2,1,0:T(8,128)(2,1)}), bf16[8,128,128]{2,1,0:T(8,128)(2,1)S(1)}, u32[]{:S(2)}, u32[]{:S(2)}) %all-to-all-start.1) | async-done | bytes 262176 | tf_op jit(solution)/shard_map/all_to_all | solution.py:209
  60.6 0.7 copy-done
  61.3 3.1 %finish.1 = bf16[384,128]{1,0:T(8,128)(2,1)} custom-call(s32[1]{0:T(128)} %bitcast.index, bf16[8,128,128]{2,1,0:T(8,128)(2,1)} %copy-done, f32[128,128]{1,0:T(8,128)} %get-tuple-element.12.inside, f32[384,128]{1,0:T(8,128)} %get-tuple-element.13.reads, f32[384,128]{1,0:T(8,128)} %get-tuple-element.14.owns, f32[1,128]{1,0:T(1,128)} %bitcast.25), custom_call_target="tpu_custom_call" | custom-call | tf_op jit(solution)/shard_map/finish/pallas_call | solution.py:260
  64.4 13.1 %all_to_all.39 = bf16[8,48,128]{2,1,0:T(8,128)(2,1)S(1)} all-to-all(bf16[8,48,128]{2,1,0:T(8,128)(2,1)} %bitcast.23), channel_id=1, replica_groups=mesh['sp_0'=8,'sp_1'=4,'tp'=8] {'tp'}, dimensions={0} | all-to-all | bytes 196608 | tf_op jit(solution)/shard_map/all_to_all | solution.py:267
  77.4 3.3 %multiply_reduce_fusion = (f32[48]{0:T(128)S(1)}, f32[48,2048]{1,0:T(8,128)S(1)}) fusion(bf16[1024,2048]{1,0:T(8,128)(2,1)} %param.25, bf16[48,2048]{1,0:T(8,128)(2,1)S(1)} %copy-done.2, bf16[8,48,128]{2,1,0:T(8,128)(2,1)S(1)} %all_to_all.39), kind=kOutput, calls=%fused_computation.14 | convolution fusion | flops 201916368 | bytes 4882624 | tf_op jit(solution)/shard_map/dot_general | solution.py:268
  80.8 0.1 multiply_convert_fusion
  80.9 0.2 broadcast_in_dim.33
  81.0 23.8 %all_to_all.40 = bf16[8,48,2048]{2,1,0:T(8,128)(2,1)S(1)} all-to-all(bf16[8,48,2048]{2,1,0:T(8,128)(2,1)S(1)} %broadcast_in_dim.33), channel_id=1, replica_groups=mesh['sp_0'=8,'sp_1'=4,'tp'=8] {'tp'}, dimensions={0} | all-to-all | bytes 3145728 | tf_op jit(solution)/shard_map/all_to_all | solution.py:209
  104.8 9.9 %all-gather.2.cloned.1.call-done = bf16[2048,2112]{1,0:T(8,128)(2,1)} async-done(((bf16[64,2112]{1,0:T(8,128)(2,1)}), bf16[2048,2112]{1,0:T(8,128)(2,1)}) %all-gather.2.cloned.1.call-update) | async-done | bytes 8650768 | tf_op jit(solution)/shard_map/all_gather | solution.py:232
  114.7 5.2 %fusion = f32[384,1408]{1,0:T(8,128)S(1)} fusion(bf16[384,2048]{1,0:T(8,128)(2,1)S(1)} %bitcast.21, bf16[2048,2112]{1,0:T(8,128)(2,1)} %all-gather.2.cloned.1.call-done), kind=kOutput, calls=%fused_computation | convolution fusion | flops 2214592512 | bytes 9502720 | tf_op jit(solution)/shard_map/dot_general | solution.py:276
  119.9 3.3 %fusion.4 = bf16[384,2048]{1,0:T(8,128)(2,1)S(1)} fusion(bf16[2048,2112]{1,0:T(8,128)(2,1)} %all-gather.2.cloned.1.call-done, f32[384,1408]{1,0:T(8,128)S(1)} %fusion), kind=kOutput, calls=%fused_computation.5 | convolution fusion | flops 1109704704 | bytes 7077888 | tf_op jit(solution)/shard_map/dot_general | solution.py:278
  123.2 26.0 %all_to_all.41 = bf16[8,48,2048]{2,1,0:T(8,128)(2,1)S(1)} all-to-all(bf16[8,48,2048]{2,1,0:T(8,128)(2,1)S(1)} %bitcast.22), channel_id=1, replica_groups=mesh['sp_0'=8,'sp_1'=4,'tp'=8] {'tp'}, dimensions={0} | all-to-all | bytes 3145728 | tf_op jit(solution)/shard_map/all_to_all | solution.py:281
  149.3 0.2 convert_reduce_fusion
  149.5 0.7 add_convert_fusion
  (9 shorter events, 0.0 us)
Async XLA Ops:
  6.5 70.9 %copy-start.2 = (bf16[48,2048]{1,0:T(8,128)(2,1)S(1)}, bf16[48,2048]{1,0:T(8,128)(2,1)}, u32[]{:S(2)}) copy-start(bf16[48,2048]{1,0:T(8,128)(2,1)} %param.15) | copy-start | bytes 589828
  6.5 108.1 %all-gather.2.cloned.1.call-start = ((), (), s32[]{:S(2)}) async-start(), calls=%async_computation.5 | async-start | bytes 9191424 | tf_op jit(solution)/shard_map/all_gather | solution.py:232
  29.2 9.7 %all-to-all-start = ((bf16[4,128,128]{2,1,0:T(8,128)(2,1)}), bf16[4,128,128]{2,1,0:T(8,128)(2,1)S(1)}, u32[]{:S(2)}, u32[]{:S(2)}) async-start(bf16[4,128,128]{2,1,0:T(8,128)(2,1)} %broadcast_in_dim.30), calls=%async_computation | async-start | bytes 262144 | tf_op jit(solution)/shard_map/all_to_all | solution.py:209
  38.9 0.7 copy-start.1
  42.9 17.6 %all-to-all-start.1 = ((bf16[8,128,128]{2,1,0:T(8,128)(2,1)}), bf16[8,128,128]{2,1,0:T(8,128)(2,1)S(1)}, u32[]{:S(2)}, u32[]{:S(2)}) async-start(bf16[8,128,128]{2,1,0:T(8,128)(2,1)} %broadcast_in_dim.31), calls=%async_computation.1 | async-start | bytes 524288 | tf_op jit(solution)/shard_map/all_to_all | solution.py:209
  60.6 0.7 copy-start
  77.4 3.3 %copy-start.3 = (f32[2048]{0:T(1024)S(1)}, f32[2048]{0:T(1024)}, u32[]{:S(2)}) copy-start(f32[2048]{0:T(1024)} %param.26) | copy-start | bytes 24580
Sparse Core Ops, SparseCore 0:
  9.9 104.7 all-gather.1

commit v2 on v1

--- a/solution.py
+++ b/solution.py
@@ -8,8 +8,6 @@
 
 HEAD = 64
 C = 64
-SP = ("sp_0", "sp_1")
-SP_TP = ("sp_0", "sp_1", "tp")
 BF = jnp.bfloat16
 F32 = jnp.float32
 
@@ -132,10 +130,12 @@
 
 def local_kernel(q, k, v, dx, lx, dco, lro, extra, reads, owns, total):
     f = lambda r: r[...].astype(F32)
-    a, b, t = local_scan(f(q), f(k), f(v), f(dx), f(lx), dco[...], lro[...], extra[...])
+    a, b, t = local_scan(f(q), f(k), f(v), f(dx), f(lx), dco[...], lro[...], extra[...].T)
     reads[...] = a
     owns[...] = b
-    total[...] = t.astype(BF)
+    out = sent(t[:HEAD], t[HEAD:])
+    for d in range(total.shape[0]):
+        total[d] = out
 
 
 def finish(reads, owns, state, gain):
@@ -155,15 +155,16 @@
         for i in range(0, len(level) - 1, 2):
             (t1, x1), (t2, x2) = level[i], level[i + 1]
             both = jnp.concatenate([t1, x1], axis=1)
-            if exact:
-                out = dot(t2.astype(BF), stacked((both.astype(BF),), masks2)[0])
-            else:
-                out = mm(split(t2), stacked(split(both), masks2))
+            out = mm(split(t2), stacked(split(both), masks2))
             nxt.append((out[:, :128], out[:, 128:] + x2))
         if len(level) % 2:
             nxt.append(level[-1])
-        level, exact = nxt, False
+        level = nxt
     return level[0]
+
+
+def eye_packed():
+    return jnp.where(iota((HEAD, 128), 0) == (iota((HEAD, 128), 1) & (HEAD - 1)), 1.0, 0.0)
 
 
 def piece(pieces, d):
@@ -171,21 +172,27 @@
     return p[:HEAD], p[HEAD:]
 
 
+def sent(trans, state):
+    return jnp.concatenate([trans - eye_packed(), state], axis=0).astype(BF)
+
+
 def earlier(pieces, count, index, masks2):
-    eye_packed = jnp.where(iota((HEAD, 128), 0) == (iota((HEAD, 128), 1) & (HEAD - 1)), 1.0, 0.0)
     level = []
     for d in range(count - 1):
         used = jnp.where(d < index, 1.0, 0.0)
         trans, state = piece(pieces, d)
-        level.append((trans * used + eye_packed * (1.0 - used), state * used))
+        level.append((trans * used + eye_packed(), state * used))
     return fold(level, masks2, True)
 
 
 def group_kernel(index, pieces, total, inside):
     masks2 = head_masks(256)
     count = pieces.shape[0]
-    t, x = fold([piece(pieces, d) for d in range(count)], masks2, True)
-    total[...] = jnp.concatenate([t, x], axis=0).astype(BF)
+    level = [piece(pieces, d) for d in range(count)]
+    t, x = fold([(t + eye_packed(), x) for t, x in level], masks2, True)
+    out = sent(t, x)
+    for d in range(total.shape[0]):
+        total[d] = out
     t, x = earlier(pieces, count, index[0], masks2)
     inside[...] = jnp.concatenate([t, x], axis=0)
 
@@ -194,7 +201,84 @@
     _, x = earlier(pieces, pieces.shape[0], index[0], head_masks(256))
     t = inside[...]
     state = mm(split(t[:HEAD]), stacked(split(x), head_masks())) + t[HEAD:]
-    mixed[...] = finish(reads[...], owns[...], state, gain[...])
+    out = finish(reads[...], owns[...], state, gain[...])
+    rows = out.shape[0] // 8
+    core = index[1]
+    parts = [[out[(2 * y + c) * rows : (2 * y + c + 1) * rows] for y in range(4)] for c in range(2)]
+    for d in range(4):
+        for y in range(4):
+            for c in range(2):
+                at = y * rows + (c ^ core) * (4 * rows)
+                mixed[d, pl.ds(pl.multiple_of(at, 16), rows)] = parts[c][y]
+
+
+def proj_kernel(index, own, sib, resid_own, resid_sib, weight, gain, mid, normed):
+    core = index[1]
+    half = own.shape[1] // 2
+    w = jnp.concatenate(
+        [
+            weight[pl.ds(pl.multiple_of((2 * y + (c ^ core)) * 128, 128), 128)]
+            for c in range(2)
+            for y in range(4)
+        ],
+        axis=0,
+    )
+    for n, resid in enumerate((resid_own, resid_sib)):
+        left = jnp.concatenate(
+            [own[y, n * half : (n + 1) * half] for y in range(4)]
+            + [sib[y, (1 - n) * half : (2 - n) * half] for y in range(4)],
+            axis=1,
+        )
+        rows = resid.shape[1]
+        m = jnp.concatenate([resid[y] for y in range(4)], axis=0).astype(F32) + dot(left, w)
+        m = m.astype(BF)
+        if n == 0:
+            for y in range(4):
+                mid[y] = m[y * rows : (y + 1) * rows]
+        m = m.astype(F32)
+        scale = lax.rsqrt(jnp.mean(m * m, axis=-1, keepdims=True) + 1e-06)
+        normed[n * half : (n + 1) * half] = (m * scale * gain[...]).astype(BF)
+
+
+def ffn_kernel(index, normed, *refs):
+    a, b, (keep, send, wa, wb, sems) = refs[:8], refs[8:12], refs[12:]
+    z, x = index[2], index[3]
+    copies_a, copies_b = [], []
+    for r in range(8):
+        copies_a.append(pltpu.make_async_copy(a[r], wa.at[(z + r) % 8], sems.at[r]))
+    for s in range(4):
+        for r in range(8):
+            copies_b.append(
+                pltpu.make_async_copy(
+                    b[s].at[r], wb.at[(z + r) % 8, (x + 4 - s) % 4], sems.at[8 + 8 * s + r]
+                )
+            )
+    for copy in copies_a + copies_b:
+        copy.start()
+    cols = wb.shape[3]
+    for copy in copies_a:
+        copy.wait()
+    both = dot(normed[...], wa[...].reshape(-1, 2 * cols))
+    gate = both[:, :cols]
+    hidden = (gate * (1.0 / (1.0 + jnp.exp(-gate))) * both[:, cols:]).astype(BF)
+    for copy in copies_b:
+        copy.wait()
+    half, rows = hidden.shape[0] // 2, hidden.shape[0] // 8
+    for k in range(8):
+        out = dot_t(hidden, wb[k].reshape(-1, cols)).astype(BF)
+        for y in range(4):
+            keep[y, k] = out[y * rows : (y + 1) * rows]
+            send[y, k] = out[half + y * rows : half + (y + 1) * rows]
+
+
+def final_kernel(index, pieces, mid, result):
+    m = mid[index[4]].astype(F32)
+    for k in range(8):
+        total = pieces[0, k].astype(F32)
+        for y in range(1, 4):
+            total = total + pieces[y, k].astype(F32)
+        at = slice(k * 256, (k + 1) * 256)
+        result[:, at] = (m[:, at] + 0.5 * total).astype(BF)
 
 
 def vmem(n):
@@ -202,11 +286,50 @@
 
 
 SMEM = pl.BlockSpec(memory_space=pltpu.SMEM)
-
-
-def from_everyone(array, axis):
-    copies = jnp.broadcast_to(array, (lax.axis_size(axis), *array.shape))
-    return lax.all_to_all(copies, axis, split_axis=0, concat_axis=0, tiled=True)
+ANY = pl.BlockSpec(memory_space=pl.ANY)
+shape = jax.ShapeDtypeStruct
+
+
+def exchanged(array, axis):
+    return lax.all_to_all(array, axis, split_axis=0, concat_axis=0, tiled=True)
+
+
+def copies(array, axis):
+    return jnp.broadcast_to(array, (lax.axis_size(axis), *array.shape))
+
+
+def shifted(array, axis, by):
+    n = lax.axis_size(axis)
+    return lax.ppermute(array, axis, [(i, (i + by) % n) for i in range(n)])
+
+
+def ring(array, axis):
+    n = lax.axis_size(axis)
+    found = {0: array}
+    up = down = array
+    for s in range(1, n // 2 + 1):
+        up = shifted(up, axis, 1)
+        found[n - s] = up
+        if s < n - s:
+            down = shifted(down, axis, -1)
+            found[s] = down
+    return [found[r] for r in range(n)]
+
+
+def call(kernel, name, out, in_specs, us, mib=16, scratch=()):
+    return pl.pallas_call(
+        kernel,
+        out_shape=out,
+        in_specs=in_specs,
+        out_specs=jax.tree.map(lambda _: vmem(1)[0], out),
+        scratch_shapes=scratch,
+        name=name,
+        compiler_params=pltpu.CompilerParams(vmem_limit_bytes=mib << 20),
+        cost_estimate=pl.CostEstimate(flops=int(us * FLOPS_US), bytes_accessed=0, transcendentals=0),
+    )
+
+
+FLOPS_US = 1e8
 
 
 def per_device(
@@ -227,17 +350,22 @@
     down_weight,
 ):
     tok = queries.shape[0]
-    shape = jax.ShapeDtypeStruct
     cols = gate_weight.shape[1]
-    weights = lax.all_gather(
-        jnp.concatenate([gate_weight, up_weight, down_weight.T], axis=1), SP, axis=0, tiled=True
-    )
-    reads, owns, total = pl.pallas_call(
+    z, x, y, c = (lax.axis_index(a).astype(jnp.int32) for a in ("z", "x", "y", "c"))
+    down = ring(down_weight.T, "z")
+    first = exchanged(copies(jnp.concatenate([gate_weight, up_weight], axis=1), "x"), "x")
+    pieces_a = ring(first, "z")
+    resid_own = exchanged(copies(resid, "y"), "y")
+    resid_sib = shifted(resid_own, "c", 1)
+    stack = jnp.stack(down)
+    pieces_b = [stack] + [shifted(stack, "x", s) for s in range(1, 4)]
+
+    reads, owns, total = call(
         local_kernel,
-        out_shape=(shape((tok, 128), F32), shape((tok, 128), F32), shape((128, 128), BF)),
-        in_specs=vmem(8),
-        out_specs=tuple(vmem(3)),
-        name="local",
+        "local",
+        (shape((tok, 128), F32), shape((tok, 128), F32), shape((4, 128, 128), BF)),
+        vmem(8),
+        18,
     )(
         queries,
         keys,
@@ -246,64 +374,79 @@
         correction_rate_input,
         decay_channel_offset[None],
         correction_rate_offset[None],
-        decay_head_extra,
-    )
-    near = from_everyone(total, "sp_1")
-    total, inside = pl.pallas_call(
+        decay_head_extra.T,
+    )
+    near = exchanged(total, "x")
+    total, inside = call(
         group_kernel,
-        out_shape=(shape((128, 128), BF), shape((128, 128), F32)),
-        in_specs=[SMEM] + vmem(1),
-        out_specs=tuple(vmem(2)),
-        name="group",
-    )(lax.axis_index("sp_1")[None], near)
-    far = from_everyone(total, "sp_0")
-    mixed = pl.pallas_call(
-        finish_kernel,
-        out_shape=shape((tok, 128), BF),
-        in_specs=[SMEM] + vmem(5),
-        out_specs=vmem(1)[0],
-        name="finish",
-    )(lax.axis_index("sp_0")[None], far, inside, reads, owns, head_norm_gain[None])
-    row_mixed = lax.all_to_all(mixed, "tp", split_axis=0, concat_axis=1, tiled=True)
-    proj = jnp.dot(row_mixed, mixer_output_weight, preferred_element_type=F32)
-    mid_f = (resid.astype(F32) + proj).astype(BF).astype(F32)
-    normed = (
-        mid_f
-        * lax.rsqrt(jnp.mean(mid_f * mid_f, axis=-1, keepdims=True) + 1e-06)
-        * feedforward_norm_gain
-    ).astype(BF)
-    rows = from_everyone(normed, "tp").reshape(tok, -1)
-    both = jnp.dot(rows, weights[:, : 2 * cols], preferred_element_type=F32)
-    hidden = (jax.nn.silu(both[:, :cols]) * both[:, cols:]).astype(BF)
-    partial = lax.dot_general(
-        hidden, weights[:, 2 * cols :], (((1,), (1,)), ((), ())), preferred_element_type=F32
-    ).astype(BF)
-    pieces = lax.all_to_all(
-        partial.reshape(8, -1, partial.shape[1]), "tp", 0, 0, tiled=True
-    )
-    down_sum = jnp.sum(pieces.astype(F32), axis=0)
-    return (mid_f + 0.5 * down_sum).astype(BF)
+        "group",
+        (shape((8, 128, 128), BF), shape((128, 128), F32)),
+        [SMEM] + vmem(1),
+        2,
+    )(jnp.stack([x]), near)
+    far = exchanged(total, "z")
+    index = jnp.stack([z, c, z, x, y])
+    mixed = call(finish_kernel, "finish", shape((4, tok, 128), BF), [SMEM] + vmem(5), 3)(
+        index, far, inside, reads, owns, head_norm_gain[None]
+    )
+    mixed_own = exchanged(mixed, "y")
+    mixed_sib = shifted(mixed_own, "c", 1)
+    mid, normed = call(
+        proj_kernel,
+        "proj",
+        (shape((4, tok // 8, 2048), BF), shape((tok, 2048), BF)),
+        [SMEM] + vmem(6),
+        4,
+        32,
+    )(
+        index,
+        mixed_own,
+        mixed_sib,
+        resid_own,
+        resid_sib,
+        mixer_output_weight,
+        feedforward_norm_gain[None],
+    )
+    part = shape((4, 8, tok // 8, 256), BF)
+    keep, send = call(
+        ffn_kernel,
+        "ffn",
+        (part, part),
+        [SMEM] + vmem(1) + [ANY] * 12,
+        8,
+        40,
+        [
+            pltpu.VMEM((8, 4, 64, 2 * cols), BF),
+            pltpu.VMEM((8, 4, 64, cols), BF),
+            pltpu.SemaphoreType.DMA((40,)),
+        ],
+    )(index, normed, *pieces_a, *pieces_b)
+    pair = (keep.astype(F32) + shifted(send, "c", 1).astype(F32)).astype(BF)
+    return call(final_kernel, "final", shape((tok // 8, 2048), BF), [SMEM] + vmem(2), 1)(
+        index, exchanged(pair, "y"), mid
+    )
 
 
 def solution(mesh):
-    torus = Mesh(mesh.devices.reshape(8, 4, mesh.shape["tp"]), ("sp_0", "sp_1", "tp"))
+    torus = Mesh(mesh.devices.reshape(8, 4, 4, 2), ("z", "x", "y", "c"))
+    sp, tp = ("z", "x"), ("y", "c")
     in_specs = (
-        P(SP_TP, None),
-        P(SP, "tp"),
-        P(SP, "tp"),
-        P(SP, "tp"),
-        P(SP, "tp"),
-        P("tp"),
-        P(SP, "tp"),
-        P(SP, "tp"),
-        P("tp"),
-        P("tp"),
+        P(sp + tp, None),
+        P(sp, tp),
+        P(sp, tp),
+        P(sp, tp),
+        P(sp, tp),
+        P(tp),
+        P(sp, tp),
+        P(sp, tp),
+        P(tp),
+        P(tp),
         P(),
         P(),
-        P(SP, "tp"),
-        P(SP, "tp"),
-        P("tp", SP),
+        P(sp, tp),
+        P(sp, tp),
+        P(tp, sp),
     )
     return jax.shard_map(
-        per_device, mesh=torus, in_specs=in_specs, out_specs=P(SP_TP, None), check_vma=False
-    )
+        per_device, mesh=torus, in_specs=in_specs, out_specs=P(sp + tp, None), check_vma=False
+    )

time: 158 us -> 174 us (1.10)
  starting transfers between devices: 13.1 us -> 47.3 us
  blocking collectives: 62.9 us -> 29.5 us
  waiting for transfers between devices: 24 us -> 49.2 us
  between operations: 13.5 us -> 0.22 us
  Pallas kernels: 22.8 us -> 35.7 us
  matrix products: 11.8 us -> 0 us
    ppermute x0 -> x20, waiting for transfers between devices: none -> 43.2 us  [shifted(): return lax.ppermute(array, axis, [(i, (i + by) % n) for i in range(n)])]
    all_to_all x3 -> x2, blocking collectives: 62.9 us -> 29.5 us  [exchanged(): return lax.all_to_all(array, axis, split_axis=0, concat_axis=0, tiled=True)]
    ppermute x0 -> x20, starting transfers between devices: none -> 28.2 us  [shifted(): return lax.ppermute(array, axis, [(i, (i + by) % n) for i in range(n)])]
    pallas_call x3 -> x6, Pallas kernels: 22.8 us -> 35.7 us  [the longest x1 16.8 us: per_device(): call(local_kernel, 'local', (shape((tok, 128), F32), shape((tok, 128), F3...]
    dot_general x3 -> x0, matrix products: 11.8 us -> none  [the longest x1 5.22 us: per_device(): both = jnp.dot(rows, weights[:, :2 * cols], preferred_element_type=F32)]
    all_gather x1 -> x0, waiting for transfers between devices: 9.86 us -> none  [per_device(): lax.all_gather(jnp.concatenate([gate_weight, up_weight, down_weight.T], a...]
    all_to_all x2 -> x4, waiting for transfers between devices: 14.2 us -> 6.02 us  [exchanged(): return lax.all_to_all(array, axis, split_axis=0, concat_axis=0, tiled=True)]
    all_to_all x2 -> x4, starting transfers between devices: 13.1 us -> 19.1 us  [exchanged(): return lax.all_to_all(array, axis, split_axis=0, concat_axis=0, tiled=True)]
  transfers between devices with their start and end apart: 3 -> 24, of which waited for: 3 -> 10; matrix products, arithmetic and copies ran while one was open for 5% -> 4% of each run, Pallas kernels for 15% -> 14%
where the time goes in v2:
time: 174 us; the launch traced here: 172 us
  waiting for transfers between devices  49.2 us (28%)
  starting transfers between devices  47.3 us (27%)
  Pallas kernels  35.7 us (21%)
  blocking collectives  29.5 us (17%)
  local copies, waits for them, and re-layouts  8.82 us (5%)
    ppermute x20, waiting for transfers between devices, shifted(): return lax.ppermute(array, axis, [(i, (i + by) % n) for i in range(n)])  43.2 us
    all_to_all x2, blocking collectives, exchanged(): return lax.all_to_all(array, axis, split_axis=0, concat_axis=0, tiled=True)  29.5 us
    ppermute x20, starting transfers between devices, shifted(): return lax.ppermute(array, axis, [(i, (i + by) % n) for i in range(n)])  28.2 us
    all_to_all x4, starting transfers between devices, exchanged(): return lax.all_to_all(array, axis, split_axis=0, concat_axis=0, tiled=True)  19.1 us
    pallas_call x1, Pallas kernels, per_device(): call(local_kernel, 'local', (shape((tok, 128), F32), shape((tok, 128), F3...  16.8 us
    pallas_call x1, Pallas kernels, per_device(): call(ffn_kernel, 'ffn', (part, part), [SMEM] + vmem(1) + [ANY] * 12, 8, 4...  11 us
    unnamed x37, local copies, waits for them, and re-layouts  6.79 us
    all_to_all x4, waiting for transfers between devices, exchanged(): return lax.all_to_all(array, axis, split_axis=0, concat_axis=0, tiled=True)  6.02 us
  transfers between devices with their start and end apart: 24, of which 10 were waited for; matrix products, arithmetic and copies ran while one was open for 4% of the time, Pallas kernels for 14%

profile of v2, /device:TPU:1, one launch (start us, length us, event | category | flops | bytes accessed | tf_op | source)
XLA Modules:
  0.0 172.1 jit_solution(31092056725769807)
XLA Ops:
  1.3 15.1 %all_to_all.30.refs_0_ = bf16[4,64,1408]{2,1,0:T(8,128)(2,1)S(1)} all-to-all(bf16[4,64,1408]{2,1,0:T(8,128)(2,1)S(1)} %broadcast_in_dim.23), channel_id=1, replica_groups=mesh['z'=8,'x'=4,'y'=4,'c'=2] {'x'}, dimensions={0} | all-to-all | bytes 1441792 | tf_op jit(solution)/shard_map/all_to_all | solution.py:294
  18.0 16.8 %local.1 = (f32[384,128]{1,0:T(8,128)S(1)}, f32[384,128]{1,0:T(8,128)S(1)}, bf16[4,128,128]{2,1,0:T(8,128)(2,1)}) custom-call(bf16[384,128]{1,0:T(8,128)(2,1)S(1)} %copy-done.3, bf16[384,128]{1,0:T(8,128)(2,1)S(1)} %copy-done.4, bf16[384,128]{1,0:T(8,128)(2,1)S(1)} %copy-done.5, bf16[384,128]{1,0:T(8,128)(2,1)S(1)} %copy-done.6, ...), custom_call_target="tpu_custom_call" | custom-call | flops 1800000000 | tf_op jit(solution)/shard_map/local/pallas_call | solution.py:363
  34.8 3.5 %all-to-all-start = ((bf16[4,128,128]{2,1,0:T(8,128)(2,1)}), bf16[4,128,128]{2,1,0:T(8,128)(2,1)S(1)}, u32[]{:S(2)}, u32[]{:S(2)}) async-start(bf16[4,128,128]{2,1,0:T(8,128)(2,1)} %get-tuple-element.14), calls=%async_computation | async-start | bytes 262144 | tf_op jit(solution)/shard_map/all_to_all | solution.py:294
  38.3 4.8 %all-to-all-done.pieces = bf16[4,128,128]{2,1,0:T(8,128)(2,1)S(1)} async-done(((bf16[4,128,128]{2,1,0:T(8,128)(2,1)}), bf16[4,128,128]{2,1,0:T(8,128)(2,1)S(1)}, u32[]{:S(2)}, u32[]{:S(2)}) %all-to-all-start) | async-done | bytes 131104 | tf_op jit(solution)/shard_map/all_to_all | solution.py:294
  44.2 7.3 %all-to-all-start.1 = ((bf16[8,128,128]{2,1,0:T(8,128)(2,1)}), bf16[8,128,128]{2,1,0:T(8,128)(2,1)S(1)}, u32[]{:S(2)}, u32[]{:S(2)}) async-start(bf16[8,128,128]{2,1,0:T(8,128)(2,1)} %get-tuple-element.15), calls=%async_computation.1 | async-start | bytes 524288 | tf_op jit(solution)/shard_map/all_to_all | solution.py:294
  51.5 2.7 %collective-permute-start.9 = (bf16[64,704]{1,0:T(8,128)(2,1)S(1)}, bf16[64,704]{1,0:T(8,128)(2,1)}, u32[]{:S(2)}, u32[]{:S(2)}) collective-permute-start(bf16[64,704]{1,0:T(8,128)(2,1)S(1)} %bitcast.32), channel_id=1, source_target_pairs={{0,224},{32,0},{64,32},{96,64},{128,96},{160,128},{192,160},{224,1... | collective-permute-start | bytes 270344 | tf_op jit(solution)/shard_map/ppermute | solution.py:303
  54.1 2.7 %collective-permute-start.2 = (bf16[4,64,1408]{2,1,0:T(8,128)(2,1)S(1)}, bf16[4,64,1408]{2,1,0:T(8,128)(2,1)}, u32[]{:S(2)}, u32[]{:S(2)}) collective-permute-start(bf16[4,64,1408]{2,1,0:T(8,128)(2,1)S(1)} %all_to_all.30.refs_0_), channel_id=1, source_target_pairs={{0,224},{32,0},{64,32},{96,64},{128,96},{160,128},{192,160},{224,1... | collective-permute-start | bytes 2162696 | tf_op jit(solution)/shard_map/ppermute | solution.py:303
  61.9 4.2 %all-to-all-start.3 = ((bf16[4,48,2048]{2,1,0:T(8,128)(2,1)}), bf16[4,48,2048]{2,1,0:T(8,128)(2,1)S(1)}, u32[]{:S(2)}, u32[]{:S(2)}) async-start(bf16[4,48,2048]{2,1,0:T(8,128)(2,1)} %broadcast_in_dim.21), calls=%async_computation.3 | async-start | bytes 1572864 | tf_op jit(solution)/shard_map/all_to_all | solution.py:294
  67.0 9.9 %collective-permute-done.10 = bf16[64,704]{1,0:T(8,128)(2,1)} collective-permute-done((bf16[64,704]{1,0:T(8,128)(2,1)}, bf16[64,704]{1,0:T(8,128)(2,1)}, u32[]{:S(2)}, u32[]{:S(2)}) %collective-permute-start.10) | collective-permute-done | bytes 90144 | tf_op jit(solution)/shard_map/ppermute | solution.py:303
  76.9 2.3 %collective-permute-start.11 = (bf16[64,704]{1,0:T(8,128)(2,1)}, bf16[64,704]{1,0:T(8,128)(2,1)S(1)}, u32[]{:S(2)}, u32[]{:S(2)}) collective-permute-start(bf16[64,704]{1,0:T(8,128)(2,1)} %collective-permute-done.10), channel_id=1, source_target_pairs={{0,224},{32,0},{64,32},{96,64},{128,96},{160,128},{192,160},{224,1... | collective-permute-start | bytes 270344 | tf_op jit(solution)/shard_map/ppermute | solution.py:303
  80.2 3.8 %collective-permute-done.14 = bf16[64,704]{1,0:T(8,128)(2,1)} collective-permute-done((bf16[64,704]{1,0:T(8,128)(2,1)S(1)}, bf16[64,704]{1,0:T(8,128)(2,1)}, u32[]{:S(2)}, u32[]{:S(2)}) %collective-permute-start.14) | collective-permute-done | bytes 90144 | tf_op jit(solution)/shard_map/ppermute | solution.py:303
  84.1 2.7 %finish.1 = bf16[4,384,128]{2,1,0:T(8,128)(2,1)} custom-call(s32[5]{0:T(128)S(1)} %stack.48.index, bf16[8,128,128]{2,1,0:T(8,128)(2,1)S(1)} %all-to-all-done.1.pieces, f32[128,128]{1,0:T(8,128)S(1)} %get-tuple-element.16.inside, f32[384,128]{1,0:T(8,128)S(1)} %get-tuple-element.17.reads, f32[384,128]{1,0:T(8,128)S(1)} %get-tuple-element.18.owns, ...), custom_call_target="tpu_custom_call" | custom-call | flops 300000000 | tf_op jit(solution)/shard_map/finish/pallas_call | solution.py:389
  86.8 4.2 %all-to-all-start.2 = ((bf16[4,384,128]{2,1,0:T(8,128)(2,1)}), bf16[4,384,128]{2,1,0:T(8,128)(2,1)S(1)}, u32[]{:S(2)}, u32[]{:S(2)}) async-start(bf16[4,384,128]{2,1,0:T(8,128)(2,1)} %finish.1), calls=%async_computation.2 | async-start | bytes 786432 | tf_op jit(solution)/shard_map/all_to_all | solution.py:294
  91.0 4.3 %collective-permute-start.1 = (bf16[4,48,2048]{2,1,0:T(8,128)(2,1)S(1)}, bf16[4,48,2048]{2,1,0:T(8,128)(2,1)S(1)}, u32[]{:S(2)}, u32[]{:S(2)}) collective-permute-start(bf16[4,48,2048]{2,1,0:T(8,128)(2,1)S(1)} %all-to-all-done.3.resid_own), channel_id=1, source_target_pairs={{0,1},{1,0},{2,3},{3,2},{4,5},{5,4},{6,7},{7,6},{8,9},{9,8},{10,11... | collective-permute-start | bytes 2359304 | tf_op jit(solution)/shard_map/ppermute | solution.py:303
  95.3 3.0 %collective-permute-start.3 = (bf16[4,64,1408]{2,1,0:T(8,128)(2,1)}, bf16[4,64,1408]{2,1,0:T(8,128)(2,1)}, u32[]{:S(2)}, u32[]{:S(2)}) collective-permute-start(bf16[4,64,1408]{2,1,0:T(8,128)(2,1)} %collective-permute-done.2.refs_1_), channel_id=1, source_target_pairs={{0,224},{32,0},{64,32},{96,64},{128,96},{160,128},{192,160},{224,1... | collective-permute-start | bytes 2162696 | tf_op jit(solution)/shard_map/ppermute | solution.py:303
  100.0 2.6 %collective-permute-start = (bf16[4,384,128]{2,1,0:T(8,128)(2,1)S(1)}, bf16[4,384,128]{2,1,0:T(8,128)(2,1)S(1)}, u32[]{:S(2)}, u32[]{:S(2)}) collective-permute-start(bf16[4,384,128]{2,1,0:T(8,128)(2,1)S(1)} %all-to-all-done.2.own), channel_id=1, source_target_pairs={{0,1},{1,0},{2,3},{3,2},{4,5},{5,4},{6,7},{7,6},{8,9},{9,8},{10,11... | collective-permute-start | bytes 1179656 | tf_op jit(solution)/shard_map/ppermute | solution.py:303
  107.2 6.7 %collective-permute-done.3.refs_2_ = bf16[4,64,1408]{2,1,0:T(8,128)(2,1)} collective-permute-done((bf16[4,64,1408]{2,1,0:T(8,128)(2,1)}, bf16[4,64,1408]{2,1,0:T(8,128)(2,1)}, u32[]{:S(2)}, u32[]{:S(2)}) %collective-permute-start.3) | collective-permute-done | bytes 720928 | tf_op jit(solution)/shard_map/ppermute | solution.py:303
  114.0 3.4 %collective-permute-start.4 = (bf16[4,64,1408]{2,1,0:T(8,128)(2,1)}, bf16[4,64,1408]{2,1,0:T(8,128)(2,1)S(1)}, u32[]{:S(2)}, u32[]{:S(2)}) collective-permute-start(bf16[4,64,1408]{2,1,0:T(8,128)(2,1)} %collective-permute-done.3.refs_2_), channel_id=1, source_target_pairs={{0,224},{32,0},{64,32},{96,64},{128,96},{160,128},{192,160},{224,1... | collective-permute-start | bytes 2162696 | tf_op jit(solution)/shard_map/ppermute | solution.py:303
  117.4 2.2 %copy-done = bf16[1024,2048]{1,0:T(8,128)(2,1)S(1)} copy-done((bf16[1024,2048]{1,0:T(8,128)(2,1)S(1)}, bf16[1024,2048]{1,0:T(8,128)(2,1)}, u32[]{:S(2)}) %copy-start) | copy-done | bytes 4194328
  119.6 2.7 %proj.1 = (bf16[4,48,2048]{2,1,0:T(8,128)(2,1)S(1)}, bf16[384,2048]{1,0:T(8,128)(2,1)S(1)}) custom-call(s32[5]{0:T(128)S(1)} %stack.48.index, bf16[4,384,128]{2,1,0:T(8,128)(2,1)S(1)} %all-to-all-done.2.own, bf16[4,384,128]{2,1,0:T(8,128)(2,1)S(1)} %collective-permute-done.sib, bf16[4,48,2048]{2,1,0:T(8,128)(2,1)S(1)} %all-to-all-done.3.resid_own, ...), custom_call_target="tpu_custom_call" | custom-call | flops 400000000 | tf_op jit(solution)/shard_map/proj/pallas_call | solution.py:394
  122.3 19.3 %collective-permute-done.16.refs_9_ = bf16[8,64,704]{2,1,0:T(8,128)(2,1)S(1)} collective-permute-done((bf16[8,64,704]{2,1,0:T(8,128)(2,1)S(1)}, bf16[8,64,704]{2,1,0:T(8,128)(2,1)S(1)}, u32[]{:S(2)}, u32[]{:S(2)}) %collective-permute-start.16) | collective-permute-done | bytes 720928 | tf_op jit(solution)/shard_map/ppermute | solution.py:303
  142.0 11.0 %ffn.1 = (bf16[4,8,48,256]{3,2,1,0:T(8,128)(2,1)S(1)}, bf16[4,8,48,256]{3,2,1,0:T(8,128)(2,1)S(1)}) custom-call(s32[5]{0:T(128)S(1)} %stack.48.index, bf16[384,2048]{1,0:T(8,128)(2,1)S(1)} %get-tuple-element.19.normed, bf16[4,64,1408]{2,1,0:T(8,128)(2,1)S(1)} %all_to_all.30.refs_0_, bf16[4,64,1408]{2,1,0:T(8,128)(2,1)} %collective-permute-done.2.refs_1_, ...), custom_call_target="tpu_custom_call" | custom-call | flops 800000000 | tf_op jit(solution)/shard_map/ffn/pallas_call | solution.py:411
  154.2 1.9 %collective-permute-done.19 = bf16[4,8,48,256]{3,2,1,0:T(8,128)(2,1)S(1)} collective-permute-done((bf16[4,8,48,256]{3,2,1,0:T(8,128)(2,1)S(1)}, bf16[4,8,48,256]{3,2,1,0:T(8,128)(2,1)S(1)}, u32[]{:S(2)}, u32[]{:S(2)}) %collective-permute-start.19) | collective-permute-done | bytes 786464 | tf_op jit(solution)/shard_map/ppermute | solution.py:303
  156.4 14.4 %all_to_all.31.pieces = bf16[4,8,48,256]{3,2,1,0:T(8,128)(2,1)S(1)} all-to-all(bf16[4,8,48,256]{3,2,1,0:T(8,128)(2,1)S(1)} %add_convert_fusion), channel_id=1, replica_groups=mesh['z'=8,'x'=4,'y'=4,'c'=2] {'y'}, dimensions={0} | all-to-all | bytes 1572864 | tf_op jit(solution)/shard_map/all_to_all | solution.py:294
  (75 shorter events, 20.5 us)
Async XLA Ops:
  16.3 40.5 %collective-permute-start.5 = (bf16[4,64,1408]{2,1,0:T(8,128)(2,1)S(1)}, bf16[4,64,1408]{2,1,0:T(8,128)(2,1)}, u32[]{:S(2)}, u32[]{:S(2)}) collective-permute-start(bf16[4,64,1408]{2,1,0:T(8,128)(2,1)S(1)} %all_to_all.30.refs_0_), channel_id=1, source_target_pairs={{0,32},{32,64},{64,96},{96,128},{128,160},{160,192},{192,224},{224... | collective-permute-start | bytes 2162696 | tf_op jit(solution)/shard_map/ppermute | solution.py:303
  34.8 8.3 %all-to-all-start = ((bf16[4,128,128]{2,1,0:T(8,128)(2,1)}), bf16[4,128,128]{2,1,0:T(8,128)(2,1)S(1)}, u32[]{:S(2)}, u32[]{:S(2)}) async-start(bf16[4,128,128]{2,1,0:T(8,128)(2,1)} %get-tuple-element.14), calls=%async_computation | async-start | bytes 262144 | tf_op jit(solution)/shard_map/all_to_all | solution.py:294
  44.2 16.7 %all-to-all-start.1 = ((bf16[8,128,128]{2,1,0:T(8,128)(2,1)}), bf16[8,128,128]{2,1,0:T(8,128)(2,1)S(1)}, u32[]{:S(2)}, u32[]{:S(2)}) async-start(bf16[8,128,128]{2,1,0:T(8,128)(2,1)} %get-tuple-element.15), calls=%async_computation.1 | async-start | bytes 524288 | tf_op jit(solution)/shard_map/all_to_all | solution.py:294
  51.5 6.6 %collective-permute-start.9 = (bf16[64,704]{1,0:T(8,128)(2,1)S(1)}, bf16[64,704]{1,0:T(8,128)(2,1)}, u32[]{:S(2)}, u32[]{:S(2)}) collective-permute-start(bf16[64,704]{1,0:T(8,128)(2,1)S(1)} %bitcast.32), channel_id=1, source_target_pairs={{0,224},{32,0},{64,32},{96,64},{128,96},{160,128},{192,160},{224,1... | collective-permute-start | bytes 270344 | tf_op jit(solution)/shard_map/ppermute | solution.py:303
  54.1 5.5 %collective-permute-start.12 = (bf16[64,704]{1,0:T(8,128)(2,1)S(1)}, bf16[64,704]{1,0:T(8,128)(2,1)S(1)}, u32[]{:S(2)}, u32[]{:S(2)}) collective-permute-start(bf16[64,704]{1,0:T(8,128)(2,1)S(1)} %bitcast.33), channel_id=1, source_target_pairs={{0,32},{32,64},{64,96},{96,128},{128,160},{160,192},{192,224},{224... | collective-permute-start | bytes 270344 | tf_op jit(solution)/shard_map/ppermute | solution.py:303
  54.1 41.1 %collective-permute-start.2 = (bf16[4,64,1408]{2,1,0:T(8,128)(2,1)S(1)}, bf16[4,64,1408]{2,1,0:T(8,128)(2,1)}, u32[]{:S(2)}, u32[]{:S(2)}) collective-permute-start(bf16[4,64,1408]{2,1,0:T(8,128)(2,1)S(1)} %all_to_all.30.refs_0_), channel_id=1, source_target_pairs={{0,224},{32,0},{64,32},{96,64},{128,96},{160,128},{192,160},{224,1... | collective-permute-start | bytes 2162696 | tf_op jit(solution)/shard_map/ppermute | solution.py:303
  56.8 41.4 %collective-permute-start.6 = (bf16[4,64,1408]{2,1,0:T(8,128)(2,1)}, bf16[4,64,1408]{2,1,0:T(8,128)(2,1)}, u32[]{:S(2)}, u32[]{:S(2)}) collective-permute-start(bf16[4,64,1408]{2,1,0:T(8,128)(2,1)} %collective-permute-done.5.refs_7_), channel_id=1, source_target_pairs={{0,32},{32,64},{64,96},{96,128},{128,160},{160,192},{192,224},{224... | collective-permute-start | bytes 2162696 | tf_op jit(solution)/shard_map/ppermute | solution.py:303
  58.0 18.8 %collective-permute-start.10 = (bf16[64,704]{1,0:T(8,128)(2,1)}, bf16[64,704]{1,0:T(8,128)(2,1)}, u32[]{:S(2)}, u32[]{:S(2)}) collective-permute-start(bf16[64,704]{1,0:T(8,128)(2,1)} %collective-permute-done.9), channel_id=1, source_target_pairs={{0,224},{32,0},{64,32},{96,64},{128,96},{160,128},{192,160},{224,1... | collective-permute-start | bytes 270344 | tf_op jit(solution)/shard_map/ppermute | solution.py:303
  59.7 19.6 %collective-permute-start.13 = (bf16[64,704]{1,0:T(8,128)(2,1)S(1)}, bf16[64,704]{1,0:T(8,128)(2,1)S(1)}, u32[]{:S(2)}, u32[]{:S(2)}) collective-permute-start(bf16[64,704]{1,0:T(8,128)(2,1)S(1)} %collective-permute-done.12), channel_id=1, source_target_pairs={{0,32},{32,64},{64,96},{96,128},{128,160},{160,192},{192,224},{224... | collective-permute-start | bytes 270344 | tf_op jit(solution)/shard_map/ppermute | solution.py:303
  61.9 24.9 %all-to-all-start.3 = ((bf16[4,48,2048]{2,1,0:T(8,128)(2,1)}), bf16[4,48,2048]{2,1,0:T(8,128)(2,1)S(1)}, u32[]{:S(2)}, u32[]{:S(2)}) async-start(bf16[4,48,2048]{2,1,0:T(8,128)(2,1)} %broadcast_in_dim.21), calls=%async_computation.3 | async-start | bytes 1572864 | tf_op jit(solution)/shard_map/all_to_all | solution.py:294
  76.9 7.2 %collective-permute-start.11 = (bf16[64,704]{1,0:T(8,128)(2,1)}, bf16[64,704]{1,0:T(8,128)(2,1)S(1)}, u32[]{:S(2)}, u32[]{:S(2)}) collective-permute-start(bf16[64,704]{1,0:T(8,128)(2,1)} %collective-permute-done.10), channel_id=1, source_target_pairs={{0,224},{32,0},{64,32},{96,64},{128,96},{160,128},{192,160},{224,1... | collective-permute-start | bytes 270344 | tf_op jit(solution)/shard_map/ppermute | solution.py:303
  79.3 4.8 %collective-permute-start.14 = (bf16[64,704]{1,0:T(8,128)(2,1)S(1)}, bf16[64,704]{1,0:T(8,128)(2,1)}, u32[]{:S(2)}, u32[]{:S(2)}) collective-permute-start(bf16[64,704]{1,0:T(8,128)(2,1)S(1)} %collective-permute-done.13), channel_id=1, source_target_pairs={{0,32},{32,64},{64,96},{96,128},{128,160},{160,192},{192,224},{224... | collective-permute-start | bytes 270344 | tf_op jit(solution)/shard_map/ppermute | solution.py:303
  84.1 14.2 %collective-permute-start.15 = (bf16[64,704]{1,0:T(8,128)(2,1)}, bf16[64,704]{1,0:T(8,128)(2,1)}, u32[]{:S(2)}, u32[]{:S(2)}) collective-permute-start(bf16[64,704]{1,0:T(8,128)(2,1)} %collective-permute-done.14), channel_id=1, source_target_pairs={{0,32},{32,64},{64,96},{96,128},{128,160},{160,192},{192,224},{224... | collective-permute-start | bytes 270344 | tf_op jit(solution)/shard_map/ppermute | solution.py:303
  86.8 13.2 %all-to-all-start.2 = ((bf16[4,384,128]{2,1,0:T(8,128)(2,1)}), bf16[4,384,128]{2,1,0:T(8,128)(2,1)S(1)}, u32[]{:S(2)}, u32[]{:S(2)}) async-start(bf16[4,384,128]{2,1,0:T(8,128)(2,1)} %finish.1), calls=%async_computation.2 | async-start | bytes 786432 | tf_op jit(solution)/shard_map/all_to_all | solution.py:294
  91.0 15.5 %collective-permute-start.1 = (bf16[4,48,2048]{2,1,0:T(8,128)(2,1)S(1)}, bf16[4,48,2048]{2,1,0:T(8,128)(2,1)S(1)}, u32[]{:S(2)}, u32[]{:S(2)}) collective-permute-start(bf16[4,48,2048]{2,1,0:T(8,128)(2,1)S(1)} %all-to-all-done.3.resid_own), channel_id=1, source_target_pairs={{0,1},{1,0},{2,3},{3,2},{4,5},{5,4},{6,7},{7,6},{8,9},{9,8},{10,11... | collective-permute-start | bytes 2359304 | tf_op jit(solution)/shard_map/ppermute | solution.py:303
  95.3 18.7 %collective-permute-start.3 = (bf16[4,64,1408]{2,1,0:T(8,128)(2,1)}, bf16[4,64,1408]{2,1,0:T(8,128)(2,1)}, u32[]{:S(2)}, u32[]{:S(2)}) collective-permute-start(bf16[4,64,1408]{2,1,0:T(8,128)(2,1)} %collective-permute-done.2.refs_1_), channel_id=1, source_target_pairs={{0,224},{32,0},{64,32},{96,64},{128,96},{160,128},{192,160},{224,1... | collective-permute-start | bytes 2162696 | tf_op jit(solution)/shard_map/ppermute | solution.py:303
  98.2 19.1 %collective-permute-start.7 = (bf16[4,64,1408]{2,1,0:T(8,128)(2,1)}, bf16[4,64,1408]{2,1,0:T(8,128)(2,1)}, u32[]{:S(2)}, u32[]{:S(2)}) collective-permute-start(bf16[4,64,1408]{2,1,0:T(8,128)(2,1)} %collective-permute-done.6.refs_6_), channel_id=1, source_target_pairs={{0,32},{32,64},{64,96},{96,128},{128,160},{160,192},{192,224},{224... | collective-permute-start | bytes 2162696 | tf_op jit(solution)/shard_map/ppermute | solution.py:303
  100.0 4.7 %collective-permute-start = (bf16[4,384,128]{2,1,0:T(8,128)(2,1)S(1)}, bf16[4,384,128]{2,1,0:T(8,128)(2,1)S(1)}, u32[]{:S(2)}, u32[]{:S(2)}) collective-permute-start(bf16[4,384,128]{2,1,0:T(8,128)(2,1)S(1)} %all-to-all-done.2.own), channel_id=1, source_target_pairs={{0,1},{1,0},{2,3},{3,2},{4,5},{5,4},{6,7},{7,6},{8,9},{9,8},{10,11... | collective-permute-start | bytes 1179656 | tf_op jit(solution)/shard_map/ppermute | solution.py:303
  104.4 37.2 %collective-permute-start.16 = (bf16[8,64,704]{2,1,0:T(8,128)(2,1)S(1)}, bf16[8,64,704]{2,1,0:T(8,128)(2,1)S(1)}, u32[]{:S(2)}, u32[]{:S(2)}) collective-permute-start(bf16[8,64,704]{2,1,0:T(8,128)(2,1)S(1)} %bitcast_dynamic-update-slice_fusion.1.refs_8_), channel_id=1, source_target_pairs={{0,8},{8,16},{16,24},{24,0},{1,9},{9,17},{17,25},{25,1},{2,10},{10... | collective-permute-start | bytes 2162696 | tf_op jit(solution)/shard_map/ppermute | solution.py:303
  104.7 36.9 %collective-permute-start.17 = (bf16[8,64,704]{2,1,0:T(8,128)(2,1)S(1)}, bf16[8,64,704]{2,1,0:T(8,128)(2,1)S(1)}, u32[]{:S(2)}, u32[]{:S(2)}) collective-permute-start(bf16[8,64,704]{2,1,0:T(8,128)(2,1)S(1)} %bitcast_dynamic-update-slice_fusion.1.refs_8_), channel_id=1, source_target_pairs={{0,16},{8,24},{16,0},{24,8},{1,17},{9,25},{17,1},{25,9},{2,18},{10... | collective-permute-start | bytes 2162696 | tf_op jit(solution)/shard_map/ppermute | solution.py:303
  106.5 35.4 %collective-permute-start.18 = (bf16[8,64,704]{2,1,0:T(8,128)(2,1)S(1)}, bf16[8,64,704]{2,1,0:T(8,128)(2,1)S(1)}, u32[]{:S(2)}, u32[]{:S(2)}) collective-permute-start(bf16[8,64,704]{2,1,0:T(8,128)(2,1)S(1)} %bitcast_dynamic-update-slice_fusion.1.refs_8_), channel_id=1, source_target_pairs={{0,24},{8,0},{16,8},{24,16},{1,25},{9,1},{17,9},{25,17},{2,26},{10... | collective-permute-start | bytes 2162696 | tf_op jit(solution)/shard_map/ppermute | solution.py:303
  114.0 28.0 %collective-permute-start.4 = (bf16[4,64,1408]{2,1,0:T(8,128)(2,1)}, bf16[4,64,1408]{2,1,0:T(8,128)(2,1)S(1)}, u32[]{:S(2)}, u32[]{:S(2)}) collective-permute-start(bf16[4,64,1408]{2,1,0:T(8,128)(2,1)} %collective-permute-done.3.refs_2_), channel_id=1, source_target_pairs={{0,224},{32,0},{64,32},{96,64},{128,96},{160,128},{192,160},{224,1... | collective-permute-start | bytes 2162696 | tf_op jit(solution)/shard_map/ppermute | solution.py:303
  117.4 24.6 %collective-permute-start.8 = (bf16[4,64,1408]{2,1,0:T(8,128)(2,1)}, bf16[4,64,1408]{2,1,0:T(8,128)(2,1)S(1)}, u32[]{:S(2)}, u32[]{:S(2)}) collective-permute-start(bf16[4,64,1408]{2,1,0:T(8,128)(2,1)} %collective-permute-done.7.refs_5_), channel_id=1, source_target_pairs={{0,32},{32,64},{64,96},{96,128},{128,160},{160,192},{192,224},{224... | collective-permute-start | bytes 2162696 | tf_op jit(solution)/shard_map/ppermute | solution.py:303
  153.0 3.1 %collective-permute-start.19 = (bf16[4,8,48,256]{3,2,1,0:T(8,128)(2,1)S(1)}, bf16[4,8,48,256]{3,2,1,0:T(8,128)(2,1)S(1)}, u32[]{:S(2)}, u32[]{:S(2)}) collective-permute-start(bf16[4,8,48,256]{3,2,1,0:T(8,128)(2,1)S(1)} %get-tuple-element.21), channel_id=1, source_target_pairs={{0,1},{1,0},{2,3},{3,2},{4,5},{5,4},{6,7},{7,6},{8,9},{9,8},{10,11... | collective-permute-start | bytes 2359304 | tf_op jit(solution)/shard_map/ppermute | solution.py:303
  (15 other events, 317.7 us)
